TPU v7x, 32 devices: a whole 2x2x4 slice. The times are simulated.
32 devices in a mesh: gr: 2 (over core), sp: 8 (over z, y), tp: 2 (over x).
Axes of the slice: x: 2, y: 2, z: 4, core: 2. Of those that a mesh axis runs over, the one named last changes fastest.
Arguments:
- tokens: bfloat16 [4, 2048, 2048], P('gr', ('sp', 'tp')), parts along dimension 0, may hold values from -6 to 6
- key_weight: bfloat16 [2048, 1024], P('sp'), may hold values from -0.125 to 0.125
- value_weight: bfloat16 [2048, 1024], P('sp'), may hold values from -0.125 to 0.125
- queries: bfloat16 [4, 1024], P('gr'), parts along dimension 0, may hold values from -6 to 6
- head_offset: float32 [16], replicated, may hold values from -14 to -3.5
- key_bias: bfloat16 [4, 2048, 16], P('gr', ('sp', 'tp')), parts along dimension 0, may hold values from -0.5 to 12.9
Outputs:
- key_cache: bfloat16 [4, 2048, 1024], P('gr', 'sp', 'tp'), parts along dimension 0
- value_cache: bfloat16 [4, 2048, 1024], P('gr', 'sp', 'tp'), parts along dimension 0
- bias_cache: bfloat16 [4, 2048, 16], P('gr', 'sp', 'tp'), parts along dimension 0
- reading: float32 [4, 1024], P('gr', 'tp'), parts along dimension 0
There are 2 independent parts, one for each index of `gr`. A program takes and returns all parts, laid end to end along the dimension named above; an argument that names none is the same for every part. Nothing has to cross between parts.
All inputs are finite; a program needn't handle non-finite values.
Results may differ from a plain program's by a relative error of at most 0.0052.
Values may be sent and summed in bfloat16 or wider, within the bound.
A program may use at most 64 MiB of HBM per device.

v0:
```python
import jax
import jax.numpy as jnp
from jax import lax
from jax.sharding import PartitionSpec as P


def carried_in(x, axis, combine, identity):
    length, position = (lax.axis_size(axis), lax.axis_index(axis))
    everything = lax.all_gather(x, axis)
    start = jnp.broadcast_to(jnp.asarray(identity, x.dtype), x.shape)

    def lap(k, before):
        at = length - 1 - k
        reached = at > position
        new = combine(before, everything[at])
        return jnp.where(reached, new, before)

    return lax.fori_loop(0, length, lap, start)


def add_terms(earlier, later):
    return earlier + later


def normalize(mixture):
    return mixture * lax.rsqrt(jnp.mean(mixture * mixture, axis=-1, keepdims=True) + 1e-06)


def per_device(tokens, key_weight, value_weight, queries, head_offset, key_bias):
    seq_count, pos_dev, model_width = tokens.shape
    head_count = head_offset.shape[0]
    kv_width = key_weight.shape[1]
    head_dim = kv_width // head_count
    score_scale = head_dim ** (-0.5)
    tp_count = lax.axis_size("tp")
    col_width = kv_width // tp_count
    col_start = lax.axis_index("tp") * col_width
    own_cols = jnp.concatenate(
        [
            lax.dynamic_slice_in_dim(key_weight, col_start, col_width, 1),
            lax.dynamic_slice_in_dim(value_weight, col_start, col_width, 1),
        ],
        axis=1,
    )
    full_cols = lax.all_gather(own_cols, "sp", axis=0, tiled=True)
    projected = jnp.einsum(
        "spd,dw->spw",
        lax.all_gather(tokens, "tp", axis=1, tiled=True),
        full_cols,
        preferred_element_type=jnp.float32,
    ).astype(jnp.bfloat16)
    key_cache = projected[:, :, :col_width]
    value_cache = projected[:, :, col_width:]
    bias_cache = lax.all_to_all(key_bias, "tp", split_axis=2, concat_axis=1, tiled=True)
    span_len = key_cache.shape[1]
    local_heads = bias_cache.shape[2]
    key_blocks = key_cache.reshape(seq_count, span_len, local_heads, head_dim)
    value_blocks = value_cache.reshape(seq_count, span_len, local_heads, head_dim)
    query_cols = lax.dynamic_slice_in_dim(queries, col_start, col_width, 1)
    query_heads = query_cols.reshape(seq_count, local_heads, head_dim)
    head_start = lax.axis_index("tp") * local_heads
    local_offset = lax.dynamic_slice_in_dim(head_offset, head_start, local_heads, 0)
    logits = (
        jnp.einsum("sphc,shc->shp", key_blocks, query_heads, preferred_element_type=jnp.float32)
        * score_scale
    )
    logits = (
        logits
        + local_offset[None, :, None]
        + jnp.transpose(bias_cache.astype(jnp.float32), (0, 2, 1))
    )
    fading = jax.nn.log_sigmoid(-logits)
    within = lax.cumsum(fading, axis=2, reverse=True) - fading
    block_total = jnp.sum(fading, axis=2)
    carried = carried_in(block_total, "sp", add_terms, jnp.zeros_like(block_total))
    weights = jnp.exp(jax.nn.log_sigmoid(logits) + within + carried[:, :, None]).astype(
        jnp.bfloat16
    )
    partial_value = jnp.einsum(
        "shp,sphc->shc", weights, value_blocks, preferred_element_type=jnp.float32
    )
    mixture = lax.psum(partial_value, "sp")
    reading = normalize(mixture).reshape(seq_count, col_width)
    return (key_cache, value_cache, bias_cache, reading)


def solution(mesh):
    in_specs = (
        P("gr", ("sp", "tp"), None),
        P("sp", None),
        P("sp", None),
        P("gr", None),
        P(),
        P("gr", ("sp", "tp"), None),
    )
    out_specs = (P("gr", "sp", "tp"), P("gr", "sp", "tp"), P("gr", "sp", "tp"), P("gr", "tp"))
    return jax.shard_map(
        per_device, mesh=mesh, in_specs=in_specs, out_specs=out_specs, check_vma=False
    )
```

profile of v0, /device:TPU:0, one launch (start us, length us, event | category | flops | bytes accessed | tf_op | source)
XLA Modules:
  0.0 179.6 jit_solution(294673093222609058)
XLA Ops:
  7.2 0.0 copy-start
  7.2 0.0 all-gather.7.cloned.1.call-start
  7.2 0.7 all-gather.7.cloned.1.call-update
  7.9 0.0 all-gather.5.cloned.1.call-start
  8.0 1.1 constant_dynamic-slice_fusion.1
  9.1 0.1 copy.28
  9.2 0.1 copy.29
  9.3 0.8 pad_maximum_fusion
  10.2 0.0 all-gather.5.cloned.1.call-update
  10.2 0.6 copy.20
  10.8 4.2 %all-to-all-start = ((bf16[2,128,16]{1,0,2:T(2,128)(2,1)}), bf16[2,128,16]{1,0,2:T(2,128)(2,1)S(1)}, u32[]{:S(2)}, u32[]{:S(2)}) async-start(bf16[2,128,16]{1,0,2:T(2,128)(2,1)} %copy.20), calls=%async_computation | async-start | bytes 16384 | tf_op jit(solution)/shard_map/all_to_all | solution.py:54
  15.1 0.1 reshape.64
  15.1 0.1 dynamic_slice.25
  15.2 30.2 %all-gather.7.cloned.1.call-done = bf16[2,256,2048]{2,1,0:T(8,128)(2,1)} async-done(((bf16[2,128,2048]{2,1,0:T(8,128)(2,1)}), bf16[2,256,2048]{2,1,0:T(8,128)(2,1)}) %all-gather.7.cloned.1.call-update) | async-done | bytes 2097168 | tf_op jit(solution)/shard_map/all_gather | solution.py:48
  45.4 77.3 %all-gather.5.cloned.1.call-done = bf16[2048,1024]{0,1:T(8,128)(2,1)} async-done(((bf16[256,1024]{0,1:T(8,128)(2,1)}), bf16[2048,1024]{0,1:T(8,128)(2,1)}) %all-gather.5.cloned.1.call-update) | async-done | bytes 4194320 | tf_op jit(solution)/shard_map/all_gather | solution.py:45
  122.7 5.2 %fusion.5 = bf16[2,256,1024]{1,2,0:T(8,128)(2,1)S(1)} fusion(bf16[2,256,2048]{2,1,0:T(8,128)(2,1)} %all-gather.7.cloned.1.call-done, bf16[2048,1024]{0,1:T(8,128)(2,1)} %all-gather.5.cloned.1.call-done), kind=kOutput, calls=%fused_computation.4 | convolution fusion | flops 2148007936 | bytes 7340032 | tf_op jit(solution)/shard_map/spd,dw->spw/dot_general | solution.py:46
  127.9 0.1 fusion.18
  128.0 0.2 fusion.19
  128.2 1.0 copy.22
  129.2 0.1 negate_bitcast_fusion
  129.3 0.2 fusion.16
  129.5 17.7 %all-gather.1 = f32[8,2,8]{2,1,0:T(2,128)S(1)} all-gather(f32[1,2,8]{2,1,0:T(2,128)S(1)} %negate_bitcast_fusion.1), channel_id=2, replica_groups=mesh['gr'=2,'sp'=8,'tp'=2] {'sp'}, dimensions={0}, use_global_device_ids=true | all-gather | bytes 576 | tf_op jit(solution)/shard_map/all_gather | solution.py:9
  147.2 0.3 while.16
  147.5 5.0 %reduce-window.6 = f32[2,8,2,128]{3,1,2,0:T(8,128)S(1)} reduce-window(f32[2,8,2,128]{3,1,2,0:T(8,128)S(1)} %get-tuple-element.150, f32[]{:T(128)} %constant.72.clone.1), window={size=1x1x1x128 pad=0_0x0_0x0_0x0_127}, to_apply=%region_0.1 | reduce-window | flops 520192 | bytes 32772 | tf_op jit(solution)/shard_map/reduce-window
  152.5 0.1 slice_reduce_fusion
  152.6 1.0 copy.23
  153.6 0.1 fusion.17
  153.7 0.2 fusion.14
  153.9 17.9 %psum.7 = f32[2,8,64]{2,1,0:T(8,128)S(1)} all-reduce(f32[2,8,64]{2,1,0:T(8,128)S(1)} %bitcast.62), channel_id=1, replica_groups=mesh['gr'=2,'sp'=8,'tp'=2] {'sp'}, use_global_device_ids=true, to_apply=%region_5.6 | all-reduce | flops 1024 | bytes 8192 | tf_op jit(solution)/shard_map/psum | solution.py:82
  171.9 0.1 multiply_reduce_fusion
  172.0 0.1 broadcast_multiply_fusion
  172.1 0.7 reshape.53
  (22 shorter events, 0.2 us)
Async XLA Ops:
  7.2 7.9 %copy-start = (bf16[2,1024]{1,0:T(2,128)(2,1)S(1)}, bf16[2,1024]{1,0:T(2,128)(2,1)}, u32[]{:S(2)}) copy-start(bf16[2,1024]{1,0:T(2,128)(2,1)} %param.11) | copy-start | bytes 12292
  7.2 38.2 %all-gather.7.cloned.1.call-start = ((), (), s32[]{:S(2)}) async-start(), calls=%async_computation.2 | async-start | bytes 3145728 | tf_op jit(solution)/shard_map/all_gather | solution.py:48
  7.9 2.3 %copy-start.2 = (bf16[2,128,16]{1,2,0:T(8,128)(2,1)S(1)}, bf16[2,128,16]{1,2,0:T(8,128)(2,1)}, u32[]{:S(2)}) copy-start(bf16[2,128,16]{1,2,0:T(8,128)(2,1)} %param.13) | copy-start | bytes 24580
  7.9 7.2 %copy-start.3 = (f32[16]{0:T(128)S(1)}, f32[16]{0:T(128)}, u32[]{:S(2)}) copy-start(f32[16]{0:T(128)} %param.12) | copy-start | bytes 196
  7.9 114.7 %all-gather.5.cloned.1.call-start = ((), (), s32[]{:S(2)}) async-start(), calls=%async_computation.1 | async-start | bytes 4718592 | tf_op jit(solution)/shard_map/all_gather | solution.py:45
  10.8 118.4 %all-to-all-start = ((bf16[2,128,16]{1,0,2:T(2,128)(2,1)}), bf16[2,128,16]{1,0,2:T(2,128)(2,1)S(1)}, u32[]{:S(2)}, u32[]{:S(2)}) async-start(bf16[2,128,16]{1,0,2:T(2,128)(2,1)} %copy.20), calls=%async_computation | async-start | bytes 16384 | tf_op jit(solution)/shard_map/all_to_all | solution.py:54
  129.3 43.5 %copy-start.1 = (bf16[2,256,8]{1,2,0:T(8,128)(2,1)}, bf16[2,256,8]{1,2,0:T(8,128)(2,1)S(1)}, u32[]{:S(2)}) copy-start(bf16[2,256,8]{1,2,0:T(8,128)(2,1)S(1)} %get-tuple-element.151) | copy-start | bytes 24580
Sparse Core Ops, SparseCore 0:
  9.5 35.8 all-gather.6
  48.0 74.6 all-gather.4
where the time goes:
time: 180 us
  waiting for transfers between devices  108 us (60%)
  blocking collectives  35.7 us (20%)
  between operations  14.2 us (8%)
  other arithmetic  6.49 us (4%)
  matrix products  5.64 us (3%)
  local copies, waits for them, and re-layouts  4.99 us (3%)
  starting transfers between devices  4.31 us (2%)
    all_gather x1, waiting for transfers between devices, per_device(): full_cols = lax.all_gather(own_cols, 'sp', axis=0, tiled=True)  77.3 us
    all_gather x1, waiting for transfers between devices, per_device(): lax.all_gather(tokens, 'tp', axis=1, tiled=True)  30.2 us
    psum x1, blocking collectives, per_device(): mixture = lax.psum(partial_value, 'sp')  17.9 us
    all_gather x1, blocking collectives, carried_in(): everything = lax.all_gather(x, axis)  17.7 us
    dot_general x1, matrix products, per_device(): jnp.einsum('spd,dw->spw', lax.all_gather(tokens, 'tp', axis=1, tiled=True...  5.22 us
    another operation x2, other arithmetic  5.02 us
    all_to_all x1, starting transfers between devices, per_device(): lax.all_to_all(key_bias, 'tp', split_axis=2, concat_axis=1, tiled=True)  4.23 us
  transfers between devices with their start and end apart: 3, of which 2 were waited for; matrix products, arithmetic and copies ran while one was open for 5% of the time, Pallas kernels for 0%

commit v1 on v0

--- a/solution.py
+++ b/solution.py
@@ -2,6 +2,15 @@
 import jax.numpy as jnp
 from jax import lax
 from jax.sharding import PartitionSpec as P
+
+
+def supply_all_sector(here_x, in_dim):
+    here_x = jnp.moveaxis(here_x, 0, in_dim)
+    step_out = here_x.shape
+    long_array = here_x.reshape(
+        *step_out[:in_dim], step_out[in_dim] * step_out[in_dim + 1], *step_out[in_dim + 2 :]
+    )
+    return long_array
 
 
 def carried_in(x, axis, combine, identity):
@@ -43,11 +52,35 @@
         axis=1,
     )
     full_cols = lax.all_gather(own_cols, "sp", axis=0, tiled=True)
-    projected = jnp.einsum(
-        "spd,dw->spw",
-        lax.all_gather(tokens, "tp", axis=1, tiled=True),
-        full_cols,
-        preferred_element_type=jnp.float32,
+
+    def see_thing_in(xs, comm_axis, dimension_no, local_values, dim_i):
+        after = lax.psum(1, axis_name=comm_axis)
+        prior, s_next, current_value = (after, lax.axis_index(comm_axis), xs.shape[dimension_no])
+        r_now = range(prior)
+        state_next = map(lambda rr: (rr, (rr + 1) % prior), r_now)
+        sides = []
+        parts_seen = list(state_next)
+        current_arr = xs
+        for i0 in range(prior):
+            r1 = (
+                current_arr
+                if i0 == prior - 1
+                else lax.ppermute(current_arr, axis_name=comm_axis, perm=parts_seen)
+            )
+            sides.append(local_values(current_arr, (s_next - i0) % prior * current_value))
+            current_arr = r1
+        sides = jnp.stack(sides, axis=0)[(s_next - jnp.arange(prior)) % prior]
+        f_next = supply_all_sector(sides, dim_i)
+        return f_next
+
+    projected = see_thing_in(
+        tokens,
+        "tp",
+        1,
+        lambda own_block, offset: jnp.einsum(
+            "spd,dw->spw", own_block, full_cols, preferred_element_type=jnp.float32
+        ),
+        1,
     ).astype(jnp.bfloat16)
     key_cache = projected[:, :, :col_width]
     value_cache = projected[:, :, col_width:]

time: 180 us -> 145 us (0.81)
  waiting for transfers between devices: 108 us -> 70.1 us
  starting transfers between devices: 4.31 us -> 6.3 us
    all_gather x1 -> x0, waiting for transfers between devices: 30.2 us -> none  [per_device(): lax.all_gather(tokens, 'tp', axis=1, tiled=True)]
    all_gather x1, waiting for transfers between devices: 77.3 us -> 70.1 us  [per_device(): full_cols = lax.all_gather(own_cols, 'sp', axis=0, tiled=True)]
    ppermute x0 -> x1, starting transfers between devices: none -> 3.03 us  [see_thing_in(): lax.ppermute(current_arr, axis_name=comm_axis, perm=parts_seen)]
    another operation x2 -> x3, other arithmetic: 5.02 us -> 5.11 us
    dot_general x1 -> x2, matrix products: 5.22 us -> 5.27 us  [per_device(): jnp.einsum('spd,dw->spw', own_block, full_cols, preferred_element_type=jn...]
  transfers between devices with their start and end apart: 3 -> 3, of which waited for: 2 -> 1; matrix products, arithmetic and copies ran while one was open for 5% -> 6% of each run, Pallas kernels for 0% -> 0%
where the time goes in v1:
time: 145 us
  waiting for transfers between devices  70.1 us (48%)
  blocking collectives  35.7 us (25%)
  between operations  14.2 us (10%)
  other arithmetic  6.62 us (5%)
  starting transfers between devices  6.3 us (4%)
  local copies, waits for them, and re-layouts  6.05 us (4%)
  matrix products  5.69 us (4%)
    all_gather x1, waiting for transfers between devices, per_device(): full_cols = lax.all_gather(own_cols, 'sp', axis=0, tiled=True)  70.1 us
    psum x1, blocking collectives, per_device(): mixture = lax.psum(partial_value, 'sp')  17.9 us
    all_gather x1, blocking collectives, carried_in(): everything = lax.all_gather(x, axis)  17.7 us
    dot_general x2, matrix products, per_device(): jnp.einsum('spd,dw->spw', own_block, full_cols, preferred_element_type=jn...  5.27 us
    another operation x2, other arithmetic  5.02 us
    all_to_all x1, starting transfers between devices, per_device(): lax.all_to_all(key_bias, 'tp', split_axis=2, concat_axis=1, tiled=True)  3.23 us
    ppermute x1, starting transfers between devices, see_thing_in(): lax.ppermute(current_arr, axis_name=comm_axis, perm=parts_seen)  3.03 us
  transfers between devices with their start and end apart: 3, of which 1 were waited for; matrix products, arithmetic and copies ran while one was open for 6% of the time, Pallas kernels for 0%

profile of v1, /device:TPU:0, one launch (start us, length us, event | category | flops | bytes accessed | tf_op | source)
XLA Modules:
  0.0 144.9 jit_solution(106371043367519002)
XLA Ops:
  7.2 0.0 all-gather.4.cloned.1.call-start
  7.2 1.1 constant_dynamic-slice_fusion.1
  8.3 0.1 copy.28
  8.4 0.1 copy.29
  8.6 0.8 pad_maximum_fusion.1
  9.4 3.0 %collective-permute-start = (bf16[2,128,2048]{2,1,0:T(8,128)(2,1)}, bf16[2,128,2048]{2,1,0:T(8,128)(2,1)S(1)}, u32[]{:S(2)}, u32[]{:S(2)}) collective-permute-start(bf16[2,128,2048]{2,1,0:T(8,128)(2,1)} %param.8), channel_id=1, source_target_pairs={{0,1},{1,0},{2,3},{3,2},{4,5},{5,4},{6,7},{7,6},{8,9},{9,8},{10,11... | collective-permute-start | bytes 3145736 | tf_op jit(solution)/shard_map/ppermute | solution.py:68
  12.5 1.3 copy.20
  13.8 3.2 %all-to-all-start = ((bf16[2,128,16]{1,0,2:T(2,128)(2,1)}), bf16[2,128,16]{1,0,2:T(2,128)(2,1)S(1)}, u32[]{:S(2)}, u32[]{:S(2)}) async-start(bf16[2,128,16]{1,0,2:T(2,128)(2,1)} %copy.20), calls=%async_computation | async-start | bytes 16384 | tf_op jit(solution)/shard_map/all_to_all | solution.py:87
  17.0 0.1 reshape.123
  17.1 0.7 dynamic_slice.25
  17.9 70.1 %all-gather.4.cloned.1.call-done = bf16[2048,1024]{0,1:T(8,128)(2,1)} async-done(((bf16[256,1024]{0,1:T(8,128)(2,1)}), bf16[2048,1024]{0,1:T(8,128)(2,1)}) %all-gather.4.cloned.1.call-update) | async-done | bytes 4194320 | tf_op jit(solution)/shard_map/all_gather | solution.py:54
  88.0 3.9 %fusion.4 = bf16[1,2,128,1024]{2,3,1,0:T(8,128)(2,1)S(1)} fusion(bf16[2,128,2048]{2,1,0:T(8,128)(2,1)} %param.8, bf16[2048,1024]{0,1:T(8,128)(2,1)} %all-gather.4.cloned.1.call-done), kind=kOutput, calls=%fused_computation.7 | convolution fusion | flops 1073741824 | bytes 5767168 | tf_op jit(solution)/shard_map/spd,dw->spw/dot_general | solution.py:80
  92.0 1.4 fusion.7
  93.3 0.1 pad_maximum_fusion
  93.4 0.7 gather_fusion
  94.2 0.5 copy.19
  94.7 0.1 fusion.22
  94.8 0.2 copy.22
  95.0 0.2 fusion.23
  95.2 0.1 negate_bitcast_fusion
  95.3 0.2 fusion.18
  95.5 17.7 %all-gather.1 = f32[8,2,8]{2,1,0:T(2,128)S(1)} all-gather(f32[1,2,8]{2,1,0:T(2,128)S(1)} %negate_bitcast_fusion.1), channel_id=2, replica_groups=mesh['gr'=2,'sp'=8,'tp'=2] {'sp'}, dimensions={0}, use_global_device_ids=true | all-gather | bytes 576 | tf_op jit(solution)/shard_map/all_gather | solution.py:18
  113.3 0.3 while.16
  113.6 5.0 %reduce-window.6 = f32[2,8,2,128]{3,1,2,0:T(8,128)S(1)} reduce-window(f32[2,8,2,128]{3,1,2,0:T(8,128)S(1)} %get-tuple-element.138, f32[]{:T(128)} %constant.88.clone.1), window={size=1x1x1x128 pad=0_0x0_0x0_0x0_127}, to_apply=%region_0.1 | reduce-window | flops 520192 | bytes 32772 | tf_op jit(solution)/shard_map/reduce-window
  118.5 0.1 slice_reduce_fusion
  118.7 0.2 copy.23
  118.9 0.1 fusion.19
  119.0 0.2 fusion.16
  119.2 17.9 %psum.7 = f32[2,8,64]{2,1,0:T(8,128)S(1)} all-reduce(f32[2,8,64]{2,1,0:T(8,128)S(1)} %bitcast.79), channel_id=1, replica_groups=mesh['gr'=2,'sp'=8,'tp'=2] {'sp'}, use_global_device_ids=true, to_apply=%region_5.6 | all-reduce | flops 1024 | bytes 8192 | tf_op jit(solution)/shard_map/psum | solution.py:115
  137.2 0.1 multiply_reduce_fusion
  137.3 0.1 broadcast_multiply_fusion
  137.3 0.7 reshape.104
  (29 shorter events, 0.3 us)
Async XLA Ops:
  7.2 9.9 %copy-start = (bf16[2,1024]{1,0:T(2,128)(2,1)S(1)}, bf16[2,1024]{1,0:T(2,128)(2,1)}, u32[]{:S(2)}) copy-start(bf16[2,1024]{1,0:T(2,128)(2,1)} %param.11) | copy-start | bytes 12292
  7.2 80.8 %all-gather.4.cloned.1.call-start = ((), (), s32[]{:S(2)}) async-start(), calls=%async_computation.1 | async-start | bytes 4718592 | tf_op jit(solution)/shard_map/all_gather | solution.py:54
  9.4 82.5 %collective-permute-start = (bf16[2,128,2048]{2,1,0:T(8,128)(2,1)}, bf16[2,128,2048]{2,1,0:T(8,128)(2,1)S(1)}, u32[]{:S(2)}, u32[]{:S(2)}) collective-permute-start(bf16[2,128,2048]{2,1,0:T(8,128)(2,1)} %param.8), channel_id=1, source_target_pairs={{0,1},{1,0},{2,3},{3,2},{4,5},{5,4},{6,7},{7,6},{8,9},{9,8},{10,11... | collective-permute-start | bytes 3145736 | tf_op jit(solution)/shard_map/ppermute | solution.py:68
  13.8 81.5 %all-to-all-start = ((bf16[2,128,16]{1,0,2:T(2,128)(2,1)}), bf16[2,128,16]{1,0,2:T(2,128)(2,1)S(1)}, u32[]{:S(2)}, u32[]{:S(2)}) async-start(bf16[2,128,16]{1,0,2:T(2,128)(2,1)} %copy.20), calls=%async_computation | async-start | bytes 16384 | tf_op jit(solution)/shard_map/all_to_all | solution.py:87
  88.0 3.9 %copy-start.4 = (bf16[2048,1024]{0,1:T(8,128)(2,1)S(1)}, bf16[2048,1024]{0,1:T(8,128)(2,1)}, u32[]{:S(2)}) copy-start(bf16[2048,1024]{0,1:T(8,128)(2,1)} %all-gather.4.cloned.1.call-done) | copy-start | bytes 12582916
  94.8 43.2 %copy-start.1 = (bf16[2,256,512]{2,1,0:T(8,128)(2,1)}, bf16[2,256,512]{2,1,0:T(8,128)(2,1)S(1)}, u32[]{:S(2)}) copy-start(bf16[2,256,512]{2,1,0:T(8,128)(2,1)S(1)} %get-tuple-element.140) | copy-start | bytes 1572868
  94.8 43.2 %copy-start.2 = (bf16[2,256,512]{2,1,0:T(8,128)(2,1)}, bf16[2,256,512]{2,1,0:T(8,128)(2,1)S(1)}, u32[]{:S(2)}) copy-start(bf16[2,256,512]{2,1,0:T(8,128)(2,1)S(1)} %get-tuple-element.141) | copy-start | bytes 1572868
  95.3 42.7 %copy-start.3 = (bf16[2,256,8]{1,2,0:T(8,128)(2,1)}, bf16[2,256,8]{1,2,0:T(8,128)(2,1)S(1)}, u32[]{:S(2)}) copy-start(bf16[2,256,8]{1,2,0:T(8,128)(2,1)S(1)} %get-tuple-element.139) | copy-start | bytes 24580
Sparse Core Ops, SparseCore 0:
  10.6 77.3 all-gather.3
